TPU v7x, 32 devices: a whole 2x2x4 slice. The times are simulated.
32 devices in a mesh: fs: 8 (over z, x), tp: 4 (over y, core).
Axes of the slice: x: 2, y: 2, z: 4, core: 2. Of those that a mesh axis runs over, the one named last changes fastest.
Arguments:
- prompt_tokens: bfloat16 [6144, 2048], P('fs', 'tp'), may hold values from -6 to 6
- norm_gain: float32 [2048], P('fs'), may hold values from 0.1 to 1.9
- up_master: float32 [2048, 4096], P('fs', 'tp'), may hold values from -6 to 6
- down_master: float32 [2048, 4096], P('fs', 'tp'), may hold values from -6 to 6
Outputs:
- serve_up: bfloat16 [2048, 4096], P(None, 'tp')
- serve_down: bfloat16 [2048, 4096], P(None, 'tp')
- mixed: bfloat16 [6144, 2048], P('fs', 'tp')
All inputs are finite; a program needn't handle non-finite values.
Results may differ from a plain program's by a relative error of at most 0.009.
Values may be sent and summed in bfloat16 or wider, within the bound.
A program may use at most 64 MiB of HBM per device.

v0:
```python
import jax
import jax.numpy as jnp
from jax import lax
from jax.sharding import PartitionSpec as P


def shards(prompt_tokens, norm_gain, up_master, down_master):
    up_folded = (norm_gain[:, None] * up_master).astype(jnp.bfloat16)
    down_cast = down_master.astype(jnp.bfloat16)
    whole = lax.all_gather(prompt_tokens, "tp", axis=1, tiled=True)
    width = whole.shape[1]
    hidden_units = up_master.shape[1] * lax.axis_size("tp")
    wide = whole.astype(jnp.float32)
    normed = (wide * lax.rsqrt(jnp.mean(wide * wide, axis=1, keepdims=True) + 1e-05)).astype(
        jnp.bfloat16
    )
    contract = (((1,), (1,)), ((), ()))
    serve_up, serve_down = (
        lax.all_gather(up_folded, "fs", axis=0, tiled=True),
        lax.all_gather(down_cast, "fs", axis=0, tiled=True),
    )
    hidden = jnp.dot(normed, serve_up, preferred_element_type=jnp.float32)
    act = jnp.square(jax.nn.relu(hidden * width ** (-0.5))).astype(jnp.bfloat16)
    product = lax.dot_general(act, serve_down, contract, preferred_element_type=jnp.float32)
    partial_value = (product * hidden_units ** (-0.5)).astype(jnp.bfloat16).astype(jnp.float32)
    mixed = lax.psum_scatter(
        partial_value.astype(jnp.bfloat16), "tp", scatter_dimension=1, tiled=True
    )
    return (serve_up, serve_down, mixed)


def solution(mesh):
    return jax.shard_map(
        shards,
        mesh=mesh,
        in_specs=(P("fs", "tp"), P("fs"), P("fs", "tp"), P("fs", "tp")),
        out_specs=(P(None, "tp"), P(None, "tp"), P("fs", "tp")),
        check_vma=False,
    )
```

profile of v0, /device:TPU:0, one launch (start us, length us, event | category | flops | bytes accessed | tf_op | source)
XLA Modules:
  0.0 252.3 jit_solution(355867088768193261)
XLA Ops:
  7.2 0.0 all-gather.8.cloned.1.call-start
  7.2 0.7 all-gather.8.cloned.1.call-update
  7.9 0.0 all-gather.4.cloned.1.call-start
  7.9 2.1 multiply_convert_fusion.2
  10.1 0.0 all-gather.4.cloned.1.call-update
  10.1 0.0 all-gather.6.cloned.1.call-start
  10.2 2.1 convert_element_type.21
  12.3 0.0 all-gather.6.cloned.1.call-update
  12.3 0.0 reduce-scatter.2.cloned.1.call-start
  12.3 28.5 %all-gather.8.cloned.1.call-done = bf16[768,2048]{1,0:T(8,128)(2,1)} async-done(((bf16[768,512]{1,0:T(8,128)(2,1)}), bf16[768,2048]{1,0:T(8,128)(2,1)}) %all-gather.8.cloned.1.call-update) | async-done | bytes 3145744 | tf_op jit(solution)/shard_map/all_gather | solution.py:10
  40.8 2.6 %fusion = f32[768]{0:T(1024)S(1)} fusion(bf16[768,2048]{1,0:T(8,128)(2,1)} %all-gather.8.cloned.1.call-done), kind=kLoop, calls=%fused_computation.2 | loop fusion | flops 4717824 | bytes 3148800 | tf_op jit(solution)/shard_map/reduce_sum | solution.py:14
  43.4 72.9 %all-gather.4.cloned.1.call-done = bf16[2048,1024]{1,0:T(8,128)(2,1)} async-done(((bf16[256,1024]{1,0:T(8,128)(2,1)}), bf16[2048,1024]{1,0:T(8,128)(2,1)}) %all-gather.4.cloned.1.call-update) | async-done | bytes 4194320 | tf_op jit(solution)/shard_map/all_gather | solution.py:19
  116.3 74.1 %all-gather.6.cloned.1.call-done = bf16[2048,1024]{1,0:T(8,128)(2,1)} async-done(((bf16[256,1024]{1,0:T(8,128)(2,1)}), bf16[2048,1024]{1,0:T(8,128)(2,1)}) %all-gather.6.cloned.1.call-update) | async-done | bytes 4194320 | tf_op jit(solution)/shard_map/all_gather | solution.py:20
  190.4 12.1 %multiply_convert_fusion = bf16[768,2048]{1,0:T(8,128)(2,1)} fusion(bf16[2048,1024]{1,0:T(8,128)(2,1)} %all-gather.6.cloned.1.call-done, bf16[2048,1024]{1,0:T(8,128)(2,1)} %all-gather.4.cloned.1.call-done, bf16[768,2048]{1,0:T(8,128)(2,1)} %all-gather.8.cloned.1.call-done, f32[768]{0:T(1024)S(1)} %add_rsqrt_fusion), kind=kOutput, calls=%fused_computation.4 | convolution fusion | flops 6453460992 | bytes 14683136 | tf_op jit(solution)/shard_map/dot_general | solution.py:24
  202.5 0.0 reduce-scatter.2.cloned.1.call-update
  202.5 36.4 %reduce-scatter.2.cloned.1.call-done = bf16[768,512]{1,0:T(8,128)(2,1)} async-done(((bf16[768,2048]{1,0:T(8,128)(2,1)}), bf16[768,512]{1,0:T(8,128)(2,1)}) %reduce-scatter.2.cloned.1.call-update) | async-done | bytes 786448 | tf_op jit(solution)/shard_map/reduce_scatter | solution.py:26
  238.9 0.0 copy-start
  238.9 4.8 %copy.9 = bf16[2048,1024]{1,0:T(8,128)(2,1)} copy(bf16[2048,1024]{1,0:T(8,128)(2,1)} %all-gather.4.cloned.1.call-done) | data formatting | bytes 8388608
  243.8 0.0 copy-done
  243.8 2.0 copy.10
  (1 shorter events, 0.0 us)
Async XLA Ops:
  7.2 33.6 %all-gather.8.cloned.1.call-start = ((), (), s32[]{:S(2)}) async-start(), calls=%async_computation.3 | async-start | bytes 3932160 | tf_op jit(solution)/shard_map/all_gather | solution.py:10
  7.9 108.4 %all-gather.4.cloned.1.call-start = ((), (), s32[]{:S(2)}) async-start(), calls=%async_computation.1 | async-start | bytes 4718592 | tf_op jit(solution)/shard_map/all_gather | solution.py:19
  10.1 180.3 %all-gather.6.cloned.1.call-start = ((), (), s32[]{:S(2)}) async-start(), calls=%async_computation.2 | async-start | bytes 4718592 | tf_op jit(solution)/shard_map/all_gather | solution.py:20
  12.3 226.7 %reduce-scatter.2.cloned.1.call-start = ((), (), s32[]{:S(2)}) async-start(), calls=%async_computation.4 | async-start | bytes 3932160 | tf_op jit(solution)/shard_map/reduce_scatter | solution.py:26
  238.9 4.8 %copy-start = (bf16[2048,1024]{1,0:T(8,128)(2,1)S(1)}, bf16[2048,1024]{1,0:T(8,128)(2,1)}, u32[]{:S(2)}) copy-start(bf16[2048,1024]{1,0:T(8,128)(2,1)} %all-gather.6.cloned.1.call-done) | copy-start | bytes 12582916
Sparse Core Ops, SparseCore 0:
  9.5 31.2 all-gather.7
  43.5 72.7 all-gather.3
  119.0 71.3 all-gather.5
  202.6 36.2 reduce-scatter.1
where the time goes:
time: 253 us; the launch traced here: 252 us
  waiting for transfers between devices  213 us (84%)
  between operations  13.8 us (5%)
  matrix products  12.1 us (5%)
  local copies, waits for them, and re-layouts  6.83 us (3%)
  other arithmetic  6.82 us (3%)
    all_gather x1, waiting for transfers between devices, shards(): lax.all_gather(down_cast, 'fs', axis=0, tiled=True)  74.1 us
    all_gather x1, waiting for transfers between devices, shards(): lax.all_gather(up_folded, 'fs', axis=0, tiled=True)  72.9 us
    reduce_scatter x1, waiting for transfers between devices, shards(): lax.psum_scatter(partial_value.astype(jnp.bfloat16), 'tp', scatter_dimens...  36.4 us
    all_gather x1, waiting for transfers between devices, shards(): whole = lax.all_gather(prompt_tokens, 'tp', axis=1, tiled=True)  28.5 us
    dot_general x1, matrix products, shards(): lax.dot_general(act, serve_down, contract, preferred_element_type=jnp.flo...  12.1 us
    unnamed x4, local copies, waits for them, and re-layouts  6.83 us
  transfers between devices with their start and end apart: 4, of which 4 were waited for; matrix products, arithmetic and copies ran while one was open for 3% of the time, Pallas kernels for 0%

commit v1 on v0

--- a/solution.py
+++ b/solution.py
@@ -1,13 +1,35 @@
+import functools
 import jax
 import jax.numpy as jnp
 from jax import lax
 from jax.sharding import PartitionSpec as P
 
 
+def try_all_state(unit, at_axis):
+    blocks_here = [unit]
+    cores_n = jax.lax.psum(1, axis_name="tp")
+    for k0 in [*range(cores_n - 1)]:
+        high = jax.lax.ppermute(
+            blocks_here[-1],
+            axis_name="tp",
+            perm=[(dev, (dev + 1) % cores_n) for dev in range(cores_n)],
+        )
+        blocks_here.append(high)
+    big = jnp.roll(
+        jnp.concatenate(blocks_here[::-1], axis=at_axis),
+        shift=(jax.lax.axis_index("tp") + 1) * unit.shape[at_axis],
+        axis=at_axis,
+    )
+    return big
+
+
+match_terms_all = functools.partial(try_all_state, at_axis=1)
+
+
 def shards(prompt_tokens, norm_gain, up_master, down_master):
     up_folded = (norm_gain[:, None] * up_master).astype(jnp.bfloat16)
     down_cast = down_master.astype(jnp.bfloat16)
-    whole = lax.all_gather(prompt_tokens, "tp", axis=1, tiled=True)
+    whole = match_terms_all(prompt_tokens)
     width = whole.shape[1]
     hidden_units = up_master.shape[1] * lax.axis_size("tp")
     wide = whole.astype(jnp.float32)

time: 253 us -> 222 us (0.88)
  waiting for transfers between devices: 213 us -> 180 us
  local copies, waits for them, and re-layouts: 6.83 us -> 10.2 us
    all_gather x1, waiting for transfers between devices: 72.9 us -> 35.2 us  [shards(): lax.all_gather(up_folded, 'fs', axis=0, tiled=True)]
    ppermute x0 -> x3, waiting for transfers between devices: none -> 34.6 us  [try_all_state(): jax.lax.ppermute(blocks_here[-1], axis_name='tp', perm=[(dev, (dev + 1) %...]
    all_gather x1 -> x0, waiting for transfers between devices: 28.5 us -> none  [shards(): whole = lax.all_gather(prompt_tokens, 'tp', axis=1, tiled=True)]
    unnamed x4 -> x15, local copies, waits for them, and re-layouts: 6.83 us -> 10.1 us
  transfers between devices with their start and end apart: 4 -> 6, of which waited for: 4 -> 6; matrix products, arithmetic and copies ran while one was open for 3% -> 2% of each run, Pallas kernels for 0% -> 0%
where the time goes in v1:
time: 222 us
  waiting for transfers between devices  180 us (81%)
  between operations  13.8 us (6%)
  matrix products  12.1 us (5%)
  local copies, waits for them, and re-layouts  10.2 us (5%)
  other arithmetic  4.99 us (2%)
    all_gather x1, waiting for transfers between devices, shards(): lax.all_gather(down_cast, 'fs', axis=0, tiled=True)  74.1 us
    reduce_scatter x1, waiting for transfers between devices, shards(): lax.psum_scatter(partial_value.astype(jnp.bfloat16), 'tp', scatter_dimens...  36.4 us
    all_gather x1, waiting for transfers between devices, shards(): lax.all_gather(up_folded, 'fs', axis=0, tiled=True)  35.2 us
    ppermute x3, waiting for transfers between devices, try_all_state(): jax.lax.ppermute(blocks_here[-1], axis_name='tp', perm=[(dev, (dev + 1) %...  34.6 us
    dot_general x1, matrix products, shards(): lax.dot_general(act, serve_down, contract, preferred_element_type=jnp.flo...  12.1 us
    unnamed x15, local copies, waits for them, and re-layouts  10.1 us
  transfers between devices with their start and end apart: 6, of which 6 were waited for; matrix products, arithmetic and copies ran while one was open for 2% of the time, Pallas kernels for 0%

profile of v1, /device:TPU:0, one launch (start us, length us, event | category | flops | bytes accessed | tf_op | source)
XLA Modules:
  0.0 222.2 jit_solution(1504854416839898904)
XLA Ops:
  7.2 0.0 copy-start.1
  7.2 0.0 all-gather.3.cloned.1.call-start
  7.2 2.2 multiply_convert_fusion.2
  9.4 0.0 all-gather.3.cloned.1.call-update
  9.5 0.0 all-gather.5.cloned.1.call-start
  9.5 2.1 convert_element_type.21
  11.6 0.0 all-gather.5.cloned.1.call-update
  11.6 0.0 reduce-scatter.2.cloned.1.call-start
  11.7 0.5 collective-permute-start
  12.2 11.8 %collective-permute-done = bf16[768,512]{1,0:T(8,128)(2,1)S(1)} collective-permute-done((bf16[768,512]{1,0:T(8,128)(2,1)}, bf16[768,512]{1,0:T(8,128)(2,1)S(1)}, u32[]{:S(2)}, u32[]{:S(2)}) %collective-permute-start) | collective-permute-done | bytes 786464 | tf_op jit(solution)/shard_map/ppermute | solution.py:12
  24.0 0.0 collective-permute-start.1
  24.1 11.4 %collective-permute-done.1 = bf16[768,512]{1,0:T(8,128)(2,1)S(1)} collective-permute-done((bf16[768,512]{1,0:T(8,128)(2,1)S(1)}, bf16[768,512]{1,0:T(8,128)(2,1)S(1)}, u32[]{:S(2)}, u32[]{:S(2)}) %collective-permute-start.1) | collective-permute-done | bytes 786464 | tf_op jit(solution)/shard_map/ppermute | solution.py:12
  35.5 0.0 collective-permute-start.2
  35.5 11.4 %collective-permute-done.2 = bf16[768,512]{1,0:T(8,128)(2,1)S(1)} collective-permute-done((bf16[768,512]{1,0:T(8,128)(2,1)S(1)}, bf16[768,512]{1,0:T(8,128)(2,1)S(1)}, u32[]{:S(2)}, u32[]{:S(2)}) %collective-permute-start.2) | collective-permute-done | bytes 786464 | tf_op jit(solution)/shard_map/ppermute | solution.py:12
  46.9 0.1 constant_dynamic-update-slice_fusion.7
  47.0 0.1 constant_dynamic-update-slice_fusion.6
  47.1 0.1 constant_dynamic-update-slice_fusion.5
  47.2 0.0 copy-done.1
  47.2 0.1 constant_dynamic-update-slice_fusion.4
  47.3 0.1 constant_dynamic-update-slice_fusion.3
  47.4 0.1 constant_dynamic-update-slice_fusion.2
  47.5 0.1 constant_dynamic-update-slice_fusion.1
  47.6 0.1 constant_dynamic-update-slice_fusion
  47.7 2.7 %copy-done.2 = bf16[768,4096]{1,0:T(8,128)(2,1)} copy-done((bf16[768,4096]{1,0:T(8,128)(2,1)}, bf16[768,4096]{1,0:T(8,128)(2,1)S(1)}, u32[]{:S(2)}) %copy-start.2) | copy-done | bytes 6291480
  50.4 0.7 fusion
  51.0 35.2 %all-gather.3.cloned.1.call-done = bf16[2048,1024]{1,0:T(8,128)(2,1)} async-done(((bf16[256,1024]{1,0:T(8,128)(2,1)}), bf16[2048,1024]{1,0:T(8,128)(2,1)}) %all-gather.3.cloned.1.call-update) | async-done | bytes 4194320 | tf_op jit(solution)/shard_map/all_gather | solution.py:41
  86.2 74.1 %all-gather.5.cloned.1.call-done = bf16[2048,1024]{1,0:T(8,128)(2,1)} async-done(((bf16[256,1024]{1,0:T(8,128)(2,1)}), bf16[2048,1024]{1,0:T(8,128)(2,1)}) %all-gather.5.cloned.1.call-update) | async-done | bytes 4194320 | tf_op jit(solution)/shard_map/all_gather | solution.py:42
  160.3 12.1 %multiply_convert_fusion = bf16[768,2048]{1,0:T(8,128)(2,1)} fusion(bf16[2048,1024]{1,0:T(8,128)(2,1)} %all-gather.5.cloned.1.call-done, bf16[2048,1024]{1,0:T(8,128)(2,1)} %all-gather.3.cloned.1.call-done, f32[768]{0:T(1024)S(1)} %add_rsqrt_fusion, bf16[768,4096]{1,0:T(8,128)(2,1)} %copy-done.2, s32[]{:T(128)S(6)} %select_n.14), kind=kOutput, calls=%fused_computation.4 | convolution fusion | flops 6453460992 | bytes 14683140 | tf_op jit(solution)/shard_map/dot_general | solution.py:46
  172.4 0.0 reduce-scatter.2.cloned.1.call-update
  172.4 36.4 %reduce-scatter.2.cloned.1.call-done = bf16[768,512]{1,0:T(8,128)(2,1)} async-done(((bf16[768,2048]{1,0:T(8,128)(2,1)}), bf16[768,512]{1,0:T(8,128)(2,1)}) %reduce-scatter.2.cloned.1.call-update) | async-done | bytes 786448 | tf_op jit(solution)/shard_map/reduce_scatter | solution.py:48
  208.8 4.8 %copy.16 = bf16[2048,1024]{1,0:T(8,128)(2,1)} copy(bf16[2048,1024]{1,0:T(8,128)(2,1)} %all-gather.3.cloned.1.call-done) | data formatting | bytes 8388608
  213.6 2.0 copy.17
  (4 shorter events, 0.0 us)
Async XLA Ops:
  7.2 40.0 %copy-start.1 = (bf16[768,512]{1,0:T(8,128)(2,1)S(1)}, bf16[768,512]{1,0:T(8,128)(2,1)}, u32[]{:S(2)}) copy-start(bf16[768,512]{1,0:T(8,128)(2,1)} %param.4) | copy-start | bytes 2359300
  7.2 79.0 %all-gather.3.cloned.1.call-start = ((), (), s32[]{:S(2)}) async-start(), calls=%async_computation.1 | async-start | bytes 4718592 | tf_op jit(solution)/shard_map/all_gather | solution.py:41
  9.5 150.8 %all-gather.5.cloned.1.call-start = ((), (), s32[]{:S(2)}) async-start(), calls=%async_computation.2 | async-start | bytes 4718592 | tf_op jit(solution)/shard_map/all_gather | solution.py:42
  11.6 197.2 %reduce-scatter.2.cloned.1.call-start = ((), (), s32[]{:S(2)}) async-start(), calls=%async_computation.3 | async-start | bytes 3932160 | tf_op jit(solution)/shard_map/reduce_scatter | solution.py:48
  11.7 12.4 %collective-permute-start = (bf16[768,512]{1,0:T(8,128)(2,1)}, bf16[768,512]{1,0:T(8,128)(2,1)S(1)}, u32[]{:S(2)}, u32[]{:S(2)}) collective-permute-start(bf16[768,512]{1,0:T(8,128)(2,1)} %param.4), channel_id=1, source_target_pairs={{0,1},{1,2},{2,3},{3,0},{4,5},{5,6},{6,7},{7,4},{8,9},{9,10},{10,1... | collective-permute-start | bytes 2359304 | tf_op jit(solution)/shard_map/ppermute | solution.py:12
  24.0 11.4 %collective-permute-start.1 = (bf16[768,512]{1,0:T(8,128)(2,1)S(1)}, bf16[768,512]{1,0:T(8,128)(2,1)S(1)}, u32[]{:S(2)}, u32[]{:S(2)}) collective-permute-start(bf16[768,512]{1,0:T(8,128)(2,1)S(1)} %collective-permute-done), channel_id=1, source_target_pairs={{0,1},{1,2},{2,3},{3,0},{4,5},{5,6},{6,7},{7,4},{8,9},{9,10},{10,1... | collective-permute-start | bytes 2359304 | tf_op jit(solution)/shard_map/ppermute | solution.py:12
  35.5 11.4 %collective-permute-start.2 = (bf16[768,512]{1,0:T(8,128)(2,1)S(1)}, bf16[768,512]{1,0:T(8,128)(2,1)S(1)}, u32[]{:S(2)}, u32[]{:S(2)}) collective-permute-start(bf16[768,512]{1,0:T(8,128)(2,1)S(1)} %collective-permute-done.1), channel_id=1, source_target_pairs={{0,1},{1,2},{2,3},{3,0},{4,5},{5,6},{6,7},{7,4},{8,9},{9,10},{10,1... | collective-permute-start | bytes 2359304 | tf_op jit(solution)/shard_map/ppermute | solution.py:12
  47.7 2.7 %copy-start.2 = (bf16[768,4096]{1,0:T(8,128)(2,1)}, bf16[768,4096]{1,0:T(8,128)(2,1)S(1)}, u32[]{:S(2)}) copy-start(bf16[768,4096]{1,0:T(8,128)(2,1)S(1)} %constant_dynamic-update-slice_fusion) | copy-start | bytes 18874372
  208.8 4.8 %copy-start = (bf16[2048,1024]{1,0:T(8,128)(2,1)S(1)}, bf16[2048,1024]{1,0:T(8,128)(2,1)}, u32[]{:S(2)}) copy-start(bf16[2048,1024]{1,0:T(8,128)(2,1)} %all-gather.5.cloned.1.call-done) | copy-start | bytes 12582916
Sparse Core Ops, SparseCore 0:
  10.7 75.4 all-gather.2
  88.9 71.3 all-gather.4
  172.5 36.2 reduce-scatter.1
